TPU v7x, 32 devices: a whole 2x2x4 slice. The times are simulated.
32 devices in a mesh: fs: 4 (over z), rep: 4 (over y, x), tp: 2 (over core).
Axes of the slice: x: 2, y: 2, z: 4, core: 2. Of those that a mesh axis runs over, the one named last changes fastest.
Arguments:
- saved_input: bfloat16 [16384, 2048], P(('fs', 'rep')), may hold values from -6 to 6
- value_cotangent: bfloat16 [16384, 4096], P(('fs', 'rep'), 'tp'), may hold values from -0.0061950684 to 0.0061950684
- factor: bfloat16 [2048, 128], P('fs'), may hold values from -1.5 to 1.5
- weight: float32 [2048, 4096], P('fs', 'tp'), may hold values from -1.2 to 1.2
- first_moment: float32 [128, 4096], P('fs', 'tp'), may hold values from -1.8 to 1.8
- second_moment: float32 [128, 4096], P('fs', 'tp'), may hold values from 0.1 to 1
Outputs:
- low_grad: float32 [128, 4096], P('fs', 'tp')
- new_first: float32 [128, 4096], P('fs', 'tp')
- new_second: float32 [128, 4096], P('fs', 'tp')
- direction: float32 [2048, 4096], P('fs', 'tp')
- new_weight: float32 [2048, 4096], P('fs', 'tp')
- new_copy: bfloat16 [2048, 4096], P('fs', 'tp')
All inputs are finite; a program needn't handle non-finite values.
Results may differ from a plain program's by a relative error of at most 0.006.
Values may be sent and summed in bfloat16 or wider, within the bound.
A program may use at most 64 MiB of HBM per device.

v0:
```python
import jax
import jax.numpy as jnp
from jax import lax
from jax.sharding import PartitionSpec as P

D = 2048
E = 4096
first_decay = 0.9
second_decay = 0.9
learn_rate = 0.05
epsilon = 1e-08


def on_device(saved_input, value_cotangent, factor, weight, first_moment, second_moment):
    factor_wide = factor.astype(jnp.float32)
    factor_whole = lax.all_gather(factor, "fs", axis=0, tiled=True)
    projected = jnp.dot(saved_input, factor_whole, preferred_element_type=jnp.float32)
    upper = projected.astype(jnp.bfloat16)
    lower = (projected - upper.astype(jnp.float32)).astype(jnp.bfloat16)
    dims = (((0,), (0,)), ((), ()))
    high_part = lax.dot_general(upper, value_cotangent, dims, preferred_element_type=jnp.float32)
    low_part = lax.dot_general(lower, value_cotangent, dims, preferred_element_type=jnp.float32)
    low_grad = lax.psum_scatter(high_part + low_part, "fs", scatter_dimension=0, tiled=True)
    low_grad = lax.psum(low_grad, "rep")
    new_first = first_decay * first_moment + (1.0 - first_decay) * low_grad
    new_second = second_decay * second_moment + (1.0 - second_decay) * low_grad * low_grad
    ratio = new_first / (jnp.sqrt(new_second) + epsilon)
    ratio_whole = lax.all_gather(ratio, "fs", axis=0, tiled=True)
    raw = jnp.dot(factor_wide, ratio_whole, precision=lax.Precision.HIGHEST)
    total = lax.psum(jnp.sum(raw * raw), ("fs", "tp"))
    spread = jnp.sqrt(total / (D * E))
    direction = raw / (spread + 1.0)
    new_weight = weight - learn_rate * direction
    return (low_grad, new_first, new_second, direction, new_weight, new_weight.astype(jnp.bfloat16))


def solution(mesh):
    placed = (
        P(("fs", "rep"), None),
        P(("fs", "rep"), "tp"),
        P("fs", None),
        P("fs", "tp"),
        P("fs", "tp"),
        P("fs", "tp"),
    )
    return jax.shard_map(
        on_device,
        mesh=mesh,
        in_specs=placed,
        out_specs=(
            P("fs", "tp"),
            P("fs", "tp"),
            P("fs", "tp"),
            P("fs", "tp"),
            P("fs", "tp"),
            P("fs", "tp"),
        ),
        check_vma=False,
    )
```

profile of v0, /device:TPU:0, one launch (start us, length us, event | category | flops | bytes accessed | tf_op | source)
XLA Modules:
  0.0 185.3 jit_solution(11213346444921834174)
XLA Ops:
  7.2 0.0 reduce-scatter.2.cloned.1.call-start
  7.2 0.0 copy-start
  7.2 17.7 %all_gather.6 = bf16[2048,128]{1,0:T(8,128)(2,1)S(1)} all-gather(bf16[512,128]{1,0:T(8,128)(2,1)} %param.8), channel_id=1, replica_groups=mesh['fs'=4,'rep'=4,'tp'=2] {'fs'}, dimensions={0}, use_global_device_ids=true | all-gather | bytes 655360 | tf_op jit(solution)/shard_map/all_gather | solution.py:16
  24.9 3.4 %fusion.6 = f32[1024,128]{1,0:T(8,128)S(1)} fusion(bf16[1024,2048]{1,0:T(8,128)(2,1)} %param.6, bf16[2048,128]{1,0:T(8,128)(2,1)S(1)} %all_gather.6), kind=kOutput, calls=%fused_computation.13 | convolution fusion | flops 536870912 | bytes 5242880 | tf_op jit(solution)/shard_map/dot_general | solution.py:17
  28.4 0.0 copy-done
  28.4 0.7 fusion.2
  29.1 0.0 copy-start.3
  29.1 0.0 copy-start.4
  29.2 1.7 convolution_add_fusion
  30.9 0.0 reduce-scatter.2.cloned.1.call-update
  30.9 0.0 all-reduce.2.cloned.1.call-start
  31.0 29.2 %reduce-scatter.2.cloned.1.call-done = f32[32,2048]{1,0:T(8,128)} async-done(((f32[128,2048]{1,0:T(8,128)}), f32[32,2048]{1,0:T(8,128)}) %reduce-scatter.2.cloned.1.call-update) | async-done | bytes 262160 | tf_op jit(solution)/shard_map/reduce_scatter | solution.py:23
  60.1 0.0 all-reduce.2.cloned.1.call-update
  60.1 0.0 all-gather.2.cloned.1.call-start
  60.2 44.5 %all-reduce.2.cloned.1.call-done = f32[32,2048]{1,0:T(8,128)} async-done(((f32[32,2048]{1,0:T(8,128)}), f32[32,2048]{1,0:T(8,128)}) %all-reduce.2.cloned.1.call-update) | async-done | bytes 262160 | tf_op jit(solution)/shard_map/psum | solution.py:24
  104.6 0.0 copy-done.3
  104.6 0.0 copy-done.4
  104.6 1.9 %add_divide_fusion = (f32[32,2048]{1,0:T(8,128)}, f32[32,2048]{1,0:T(8,128)}, f32[32,2048]{1,0:T(8,128)}) fusion(f32[32,2048]{1,0:T(8,128)} %all-reduce.2.cloned.1.call-done, f32[32,2048]{1,0:T(8,128)S(1)} %copy-done.3, f32[32,2048]{1,0:T(8,128)S(1)} %copy-done.4), kind=kLoop, calls=%fused_computation.8 | loop fusion | flops 524288 | bytes 1572864 | tf_op jit(solution)/shard_map/div | solution.py:27
  106.5 0.0 all-gather.2.cloned.1.call-update
  106.6 0.0 copy-start.2
  106.6 5.4 %copy.12 = f32[512,2048]{0,1:T(8,128)} copy(f32[512,2048]{1,0:T(8,128)} %param.9) | data formatting | bytes 8388608 | tf_op args[3]
  112.0 22.8 %all-gather.2.cloned.1.call-done = f32[128,2048]{1,0:T(8,128)} async-done(((f32[32,2048]{1,0:T(8,128)}), f32[128,2048]{1,0:T(8,128)}) %all-gather.2.cloned.1.call-update) | async-done | bytes 1048592 | tf_op jit(solution)/shard_map/all_gather | solution.py:28
  134.8 0.0 copy-done.2
  134.8 6.0 %multiply_reduce_fusion = (f32[]{:T(128)}, f32[2048,512]{1,0:T(8,128)}) fusion(f32[128,2048]{1,0:T(8,128)} %all-gather.2.cloned.1.call-done, bf16[512,128]{1,0:T(8,128)(2,1)S(1)} %copy-done.2), kind=kOutput, calls=%fused_computation.2 | convolution fusion | flops 1612709888 | bytes 5373956 | tf_op jit(solution)/shard_map/dot_general | solution.py:29
  140.8 15.3 %psum.15 = f32[]{:T(128)} all-reduce(f32[]{:T(128)} %get-tuple-element.18), channel_id=1, replica_groups=mesh['fs'=4,'rep'=4,'tp'=2] {'fs','tp'}, use_global_device_ids=true, to_apply=%region_3.0 | all-reduce | flops 1 | bytes 8 | tf_op jit(solution)/shard_map/psum | solution.py:30
  156.7 8.3 %fusion.4 = (bf16[512,2048]{0,1:T(8,128)(2,1)S(1)}, f32[512,2048]{0,1:T(8,128)}, f32[512,2048]{0,1:T(8,128)}) fusion(f32[512,2048]{0,1:T(8,128)} %copy.12, f32[2048,512]{1,0:T(8,128)} %get-tuple-element.19, f32[]{:T(128)S(6)} %add.29), kind=kLoop, calls=%fused_computation.12 | loop fusion | flops 4194304 | bytes 18874372 | tf_op jit(solution)/shard_map/convert_element_type | solution.py:34
  165.0 2.4 %copy.15 = bf16[512,2048]{1,0:T(8,128)(2,1)} copy(bf16[512,2048]{0,1:T(8,128)(2,1)S(1)} %get-tuple-element.12) | data formatting | bytes 4194304
  167.4 5.3 %copy.14 = f32[512,2048]{1,0:T(8,128)} copy(f32[512,2048]{0,1:T(8,128)} %get-tuple-element.13) | data formatting | bytes 8388608
  172.7 0.0 copy-start.1
  172.7 5.4 %copy.13 = f32[512,2048]{1,0:T(8,128)} copy(f32[512,2048]{0,1:T(8,128)} %get-tuple-element.14) | data formatting | bytes 8388608
  178.1 0.0 copy-done.1
  178.1 0.7 copy.17
Async XLA Ops:
  7.2 52.9 %reduce-scatter.2.cloned.1.call-start = ((), (), s32[]{:S(2)}) async-start(), calls=%async_computation.1 | async-start | bytes 1310720 | tf_op jit(solution)/shard_map/reduce_scatter | solution.py:23
  7.2 21.2 %copy-start = (bf16[1024,2048]{1,0:T(8,128)(2,1)S(1)}, bf16[1024,2048]{1,0:T(8,128)(2,1)}, u32[]{:S(2)}) copy-start(bf16[1024,2048]{1,0:T(8,128)(2,1)} %param.7) | copy-start | bytes 12582916
  29.1 75.5 %copy-start.3 = (f32[32,2048]{1,0:T(8,128)S(1)}, f32[32,2048]{1,0:T(8,128)}, u32[]{:S(2)}) copy-start(f32[32,2048]{1,0:T(8,128)} %param.11) | copy-start | bytes 786436
  29.1 75.5 %copy-start.4 = (f32[32,2048]{1,0:T(8,128)S(1)}, f32[32,2048]{1,0:T(8,128)}, u32[]{:S(2)}) copy-start(f32[32,2048]{1,0:T(8,128)} %param.10) | copy-start | bytes 786436
  30.9 73.7 %all-reduce.2.cloned.1.call-start = ((), (), s32[]{:S(2)}) async-start(), calls=%async_computation.2 | async-start | bytes 524288 | tf_op jit(solution)/shard_map/psum | solution.py:24
  60.1 74.7 %all-gather.2.cloned.1.call-start = ((), (), s32[]{:S(2)}) async-start(), calls=%async_computation.3 | async-start | bytes 1310720 | tf_op jit(solution)/shard_map/all_gather | solution.py:28
  106.6 28.2 %copy-start.2 = (bf16[512,128]{1,0:T(8,128)(2,1)S(1)}, bf16[512,128]{1,0:T(8,128)(2,1)}, u32[]{:S(2)}) copy-start(bf16[512,128]{1,0:T(8,128)(2,1)} %param.8) | copy-start | bytes 393220
  172.7 5.4 %copy-start.1 = (f32[32,2048]{1,0:T(8,128)S(1)}, f32[32,2048]{1,0:T(8,128)}, u32[]{:S(2)}) copy-start(f32[32,2048]{1,0:T(8,128)} %all-reduce.2.cloned.1.call-done) | copy-start | bytes 786436
Sparse Core Ops, SparseCore 0:
  31.0 29.0 reduce-scatter.1
  63.0 41.5 all-reduce.1
  106.8 27.9 all-gather.1
where the time goes:
time: 186 us; the launch traced here: 185 us
  waiting for transfers between devices  96.5 us (52%)
  blocking collectives  33 us (18%)
  local copies, waits for them, and re-layouts  19.2 us (10%)
  between operations  14.5 us (8%)
  matrix products  11.9 us (6%)
  other arithmetic  10.2 us (5%)
    psum x1, waiting for transfers between devices, on_device(): low_grad = lax.psum(low_grad, 'rep')  44.5 us
    reduce_scatter x1, waiting for transfers between devices, on_device(): lax.psum_scatter(high_part + low_part, 'fs', scatter_dimension=0, tiled=T...  29.2 us
    all_gather x1, waiting for transfers between devices, on_device(): ratio_whole = lax.all_gather(ratio, 'fs', axis=0, tiled=True)  22.8 us
    unnamed x15, local copies, waits for them, and re-layouts  19.2 us
    all_gather x1, blocking collectives, on_device(): factor_whole = lax.all_gather(factor, 'fs', axis=0, tiled=True)  17.7 us
    psum x1, blocking collectives, on_device(): total = lax.psum(jnp.sum(raw * raw), ('fs', 'tp'))  15.3 us
    convert_element_type x1, other arithmetic, on_device(): new_weight.astype(jnp.bfloat16)  8.28 us
    dot_general x1, matrix products, on_device(): raw = jnp.dot(factor_wide, ratio_whole, precision=lax.Precision.HIGHEST)  5.95 us
  transfers between devices with their start and end apart: 3, of which 3 were waited for; matrix products, arithmetic and copies ran while one was open for 3% of the time, Pallas kernels for 0%

commit v1 on v0

--- a/solution.py
+++ b/solution.py
@@ -21,7 +21,9 @@
     high_part = lax.dot_general(upper, value_cotangent, dims, preferred_element_type=jnp.float32)
     low_part = lax.dot_general(lower, value_cotangent, dims, preferred_element_type=jnp.float32)
     low_grad = lax.psum_scatter(high_part + low_part, "fs", scatter_dimension=0, tiled=True)
-    low_grad = lax.psum(low_grad, "rep")
+    low_grad = low_grad
+    for hop in (1, 2):
+        low_grad = low_grad + lax.ppermute(low_grad, "rep", [(dev, dev ^ hop) for dev in range(4)])
     new_first = first_decay * first_moment + (1.0 - first_decay) * low_grad
     new_second = second_decay * second_moment + (1.0 - second_decay) * low_grad * low_grad
     ratio = new_first / (jnp.sqrt(new_second) + epsilon)

time: 186 us -> 155 us (0.83)
  waiting for transfers between devices: 96.5 us -> 62.8 us
  starting transfers between devices: 0.12 us -> 3.09 us
    psum x1 -> x0, waiting for transfers between devices: 44.5 us -> none  [on_device(): low_grad = lax.psum(low_grad, 'rep')]
    ppermute x0 -> x2, waiting for transfers between devices: none -> 11.7 us  [on_device(): lax.ppermute(low_grad, 'rep', [(dev, dev ^ hop) for dev in range(4)])]
    ppermute x0 -> x2, starting transfers between devices: none -> 3.01 us  [on_device(): lax.ppermute(low_grad, 'rep', [(dev, dev ^ hop) for dev in range(4)])]
    unnamed x15 -> x12, local copies, waits for them, and re-layouts: 19.2 us -> 18.4 us
  transfers between devices with their start and end apart: 3 -> 4, of which waited for: 3 -> 4; matrix products, arithmetic and copies ran while one was open for 3% -> 3% of each run, Pallas kernels for 0% -> 0%
where the time goes in v1:
time: 155 us; the launch traced here: 154 us
  waiting for transfers between devices  62.8 us (41%)
  blocking collectives  33 us (21%)
  local copies, waits for them, and re-layouts  18.4 us (12%)
  between operations  14.8 us (10%)
  matrix products  11.8 us (8%)
  other arithmetic  10.3 us (7%)
  starting transfers between devices  3.09 us (2%)
    reduce_scatter x1, waiting for transfers between devices, on_device(): lax.psum_scatter(high_part + low_part, 'fs', scatter_dimension=0, tiled=T...  29.2 us
    all_gather x1, waiting for transfers between devices, on_device(): ratio_whole = lax.all_gather(ratio, 'fs', axis=0, tiled=True)  21.9 us
    unnamed x12, local copies, waits for them, and re-layouts  18.4 us
    all_gather x1, blocking collectives, on_device(): factor_whole = lax.all_gather(factor, 'fs', axis=0, tiled=True)  17.7 us
    psum x1, blocking collectives, on_device(): total = lax.psum(jnp.sum(raw * raw), ('fs', 'tp'))  15.3 us
    ppermute x2, waiting for transfers between devices, on_device(): lax.ppermute(low_grad, 'rep', [(dev, dev ^ hop) for dev in range(4)])  11.7 us
    convert_element_type x1, other arithmetic, on_device(): new_weight.astype(jnp.bfloat16)  8.28 us
    dot_general x1, matrix products, on_device(): raw = jnp.dot(factor_wide, ratio_whole, precision=lax.Precision.HIGHEST)  5.95 us
  transfers between devices with their start and end apart: 4, of which 4 were waited for; matrix products, arithmetic and copies ran while one was open for 3% of the time, Pallas kernels for 0%

profile of v1, /device:TPU:0, one launch (start us, length us, event | category | flops | bytes accessed | tf_op | source)
XLA Modules:
  0.0 154.3 jit_solution(117610168198061486)
XLA Ops:
  7.2 0.0 reduce-scatter.2.cloned.1.call-start
  7.2 0.0 copy-start
  7.2 17.7 %all_gather.6 = bf16[2048,128]{1,0:T(8,128)(2,1)S(1)} all-gather(bf16[512,128]{1,0:T(8,128)(2,1)} %param.8), channel_id=1, replica_groups=mesh['fs'=4,'rep'=4,'tp'=2] {'fs'}, dimensions={0}, use_global_device_ids=true | all-gather | bytes 655360 | tf_op jit(solution)/shard_map/all_gather | solution.py:16
  24.9 3.4 %fusion.6 = f32[1024,128]{1,0:T(8,128)S(1)} fusion(bf16[1024,2048]{1,0:T(8,128)(2,1)} %param.6, bf16[2048,128]{1,0:T(8,128)(2,1)S(1)} %all_gather.6), kind=kOutput, calls=%fused_computation.13 | convolution fusion | flops 536870912 | bytes 5242880 | tf_op jit(solution)/shard_map/dot_general | solution.py:17
  28.4 0.0 copy-done
  28.4 0.7 fusion.2
  29.1 0.0 copy-start.2
  29.1 0.0 copy-start.3
  29.2 1.7 %convolution_add_fusion = f32[128,2048]{1,0:T(8,128)} fusion(f32[128,2048]{1,0:T(8,128)S(1)} %fusion.2, bf16[1024,2048]{1,0:T(8,128)(2,1)S(1)} %copy-done, f32[1024,128]{1,0:T(8,128)S(1)} %fusion.6), kind=kOutput, calls=%fused_computation.3 | convolution fusion | flops 537657344 | bytes 6815744 | tf_op jit(solution)/shard_map/dot_general | solution.py:22
  30.9 0.0 reduce-scatter.2.cloned.1.call-update
  30.9 0.0 all-gather.2.cloned.1.call-start
  31.0 29.2 %reduce-scatter.2.cloned.1.call-done = f32[32,2048]{1,0:T(8,128)} async-done(((f32[128,2048]{1,0:T(8,128)}), f32[32,2048]{1,0:T(8,128)}) %reduce-scatter.2.cloned.1.call-update) | async-done | bytes 262160 | tf_op jit(solution)/shard_map/reduce_scatter | solution.py:23
  60.1 1.5 collective-permute-start
  61.6 6.4 %collective-permute-done = f32[32,2048]{1,0:T(8,128)S(1)} collective-permute-done((f32[32,2048]{1,0:T(8,128)}, f32[32,2048]{1,0:T(8,128)S(1)}, u32[]{:S(2)}, u32[]{:S(2)}) %collective-permute-start) | collective-permute-done | bytes 262176 | tf_op jit(solution)/shard_map/ppermute | solution.py:26
  68.0 1.0 add.29
  69.0 1.5 %collective-permute-start.1 = (f32[32,2048]{1,0:T(8,128)S(1)}, f32[32,2048]{1,0:T(8,128)S(1)}, u32[]{:S(2)}, u32[]{:S(2)}) collective-permute-start(f32[32,2048]{1,0:T(8,128)S(1)} %add.29), channel_id=1, source_target_pairs={{0,4},{2,6},{4,0},{6,2},{1,5},{3,7},{5,1},{7,3},{8,12},{10,14},{12... | collective-permute-start | bytes 786440 | tf_op jit(solution)/shard_map/ppermute | solution.py:26
  70.5 5.3 %collective-permute-done.1 = f32[32,2048]{1,0:T(8,128)S(1)} collective-permute-done((f32[32,2048]{1,0:T(8,128)S(1)}, f32[32,2048]{1,0:T(8,128)S(1)}, u32[]{:S(2)}, u32[]{:S(2)}) %collective-permute-start.1) | collective-permute-done | bytes 262176 | tf_op jit(solution)/shard_map/ppermute | solution.py:26
  75.8 0.0 copy-done.2
  75.8 0.0 copy-done.3
  75.8 1.0 add_divide_fusion
  76.8 0.0 all-gather.2.cloned.1.call-update
  76.9 0.0 copy-start.1
  76.9 5.4 %copy.12 = f32[512,2048]{0,1:T(8,128)} copy(f32[512,2048]{1,0:T(8,128)} %param.9) | data formatting | bytes 8388608 | tf_op args[3]
  82.3 21.9 %all-gather.2.cloned.1.call-done = f32[128,2048]{1,0:T(8,128)} async-done(((f32[32,2048]{1,0:T(8,128)}), f32[128,2048]{1,0:T(8,128)}) %all-gather.2.cloned.1.call-update) | async-done | bytes 1048592 | tf_op jit(solution)/shard_map/all_gather | solution.py:30
  104.2 0.0 copy-done.1
  104.2 6.0 %multiply_reduce_fusion = (f32[]{:T(128)}, f32[2048,512]{1,0:T(8,128)}) fusion(f32[128,2048]{1,0:T(8,128)} %all-gather.2.cloned.1.call-done, bf16[512,128]{1,0:T(8,128)(2,1)S(1)} %copy-done.1), kind=kOutput, calls=%fused_computation.2 | convolution fusion | flops 1612709888 | bytes 5373956 | tf_op jit(solution)/shard_map/dot_general | solution.py:31
  110.1 15.3 %psum.7 = f32[]{:T(128)} all-reduce(f32[]{:T(128)} %get-tuple-element.19), channel_id=1, replica_groups=mesh['fs'=4,'rep'=4,'tp'=2] {'fs','tp'}, use_global_device_ids=true, to_apply=%region_2.0 | all-reduce | flops 1 | bytes 8 | tf_op jit(solution)/shard_map/psum | solution.py:32
  126.1 8.3 %fusion.4 = (bf16[512,2048]{0,1:T(8,128)(2,1)S(1)}, f32[512,2048]{0,1:T(8,128)}, f32[512,2048]{0,1:T(8,128)}) fusion(f32[512,2048]{0,1:T(8,128)} %copy.12, f32[2048,512]{1,0:T(8,128)} %get-tuple-element.20, f32[]{:T(128)S(6)} %add.35), kind=kLoop, calls=%fused_computation.12 | loop fusion | flops 4194304 | bytes 18874372 | tf_op jit(solution)/shard_map/convert_element_type | solution.py:36
  134.4 2.4 %copy.15 = bf16[512,2048]{1,0:T(8,128)(2,1)} copy(bf16[512,2048]{0,1:T(8,128)(2,1)S(1)} %get-tuple-element.12) | data formatting | bytes 4194304
  136.8 5.3 %copy.14 = f32[512,2048]{1,0:T(8,128)} copy(f32[512,2048]{0,1:T(8,128)} %get-tuple-element.13) | data formatting | bytes 8388608
  142.1 5.3 %copy.13 = f32[512,2048]{1,0:T(8,128)} copy(f32[512,2048]{0,1:T(8,128)} %get-tuple-element.14) | data formatting | bytes 8388608
Async XLA Ops:
  7.2 52.9 %reduce-scatter.2.cloned.1.call-start = ((), (), s32[]{:S(2)}) async-start(), calls=%async_computation.1 | async-start | bytes 1310720 | tf_op jit(solution)/shard_map/reduce_scatter | solution.py:23
  7.2 21.2 %copy-start = (bf16[1024,2048]{1,0:T(8,128)(2,1)S(1)}, bf16[1024,2048]{1,0:T(8,128)(2,1)}, u32[]{:S(2)}) copy-start(bf16[1024,2048]{1,0:T(8,128)(2,1)} %param.7) | copy-start | bytes 12582916
  29.1 46.7 %copy-start.2 = (f32[32,2048]{1,0:T(8,128)S(1)}, f32[32,2048]{1,0:T(8,128)}, u32[]{:S(2)}) copy-start(f32[32,2048]{1,0:T(8,128)} %param.11) | copy-start | bytes 786436
  29.1 46.7 %copy-start.3 = (f32[32,2048]{1,0:T(8,128)S(1)}, f32[32,2048]{1,0:T(8,128)}, u32[]{:S(2)}) copy-start(f32[32,2048]{1,0:T(8,128)} %param.10) | copy-start | bytes 786436
  30.9 73.3 %all-gather.2.cloned.1.call-start = ((), (), s32[]{:S(2)}) async-start(), calls=%async_computation.2 | async-start | bytes 1310720 | tf_op jit(solution)/shard_map/all_gather | solution.py:30
  60.1 7.9 %collective-permute-start = (f32[32,2048]{1,0:T(8,128)}, f32[32,2048]{1,0:T(8,128)S(1)}, u32[]{:S(2)}, u32[]{:S(2)}) collective-permute-start(f32[32,2048]{1,0:T(8,128)} %reduce-scatter.2.cloned.1.call-done), channel_id=1, source_target_pairs={{0,2},{2,0},{4,6},{6,4},{1,3},{3,1},{5,7},{7,5},{8,10},{10,8},{12,... | collective-permute-start | bytes 786440 | tf_op jit(solution)/shard_map/ppermute | solution.py:26
  69.0 6.8 %collective-permute-start.1 = (f32[32,2048]{1,0:T(8,128)S(1)}, f32[32,2048]{1,0:T(8,128)S(1)}, u32[]{:S(2)}, u32[]{:S(2)}) collective-permute-start(f32[32,2048]{1,0:T(8,128)S(1)} %add.29), channel_id=1, source_target_pairs={{0,4},{2,6},{4,0},{6,2},{1,5},{3,7},{5,1},{7,3},{8,12},{10,14},{12... | collective-permute-start | bytes 786440 | tf_op jit(solution)/shard_map/ppermute | solution.py:26
  76.9 27.3 %copy-start.1 = (bf16[512,128]{1,0:T(8,128)(2,1)S(1)}, bf16[512,128]{1,0:T(8,128)(2,1)}, u32[]{:S(2)}) copy-start(bf16[512,128]{1,0:T(8,128)(2,1)} %param.8) | copy-start | bytes 393220
Sparse Core Ops, SparseCore 0:
  31.0 29.0 reduce-scatter.1
  77.0 27.1 all-gather.1
